TPU v7x, 512 devices: a whole 4x8x8 slice. The times are simulated.
512 devices in a mesh: sp: 32 (over z, x), tp: 16 (over y, core).
Axes of the slice: x: 4, y: 8, z: 8, core: 2. Of those that a mesh axis runs over, the one named last changes fastest.
Arguments:
- resid: bfloat16 [4096, 2048], P('sp'), may hold values from -6 to 6
- norm_gain: float32 [2048], replicated, may hold values from 0.1 to 1.9
- cotangent: bfloat16 [4096, 2048], P('sp'), may hold values from -6 to 6
- route_ids: int32 [4096, 2], P('sp'), may hold values from 0 to 31, all different within a row; in each aligned block of 128 rows (0 to 127, 128 to 255, ...) at most 12 rows name the same one
- route_weight: float32 [4096, 2], P('sp'), may hold values from 0.25 to 2.25
- expert_gate: bfloat16 [32, 2048, 2048], P('sp', None, 'tp'), may hold values from -0.125 to 0.125
- expert_up: bfloat16 [32, 2048, 2048], P('sp', None, 'tp'), may hold values from -0.125 to 0.125
- expert_down: bfloat16 [32, 2048, 2048], P('sp', 'tp'), may hold values from -0.125 to 0.125
- out_proj: bfloat16 [2048, 4096], P('sp', 'tp'), may hold values from -0.09375 to 0.09375
- mixed: bfloat16 [4096, 4096], P('sp', 'tp'), may hold values from -6 to 6
- query: bfloat16 [4096, 2048], P('sp', 'tp'), may hold values from -6 to 6
- key: bfloat16 [4096, 2048], P('sp', 'tp'), may hold values from -1.5 to 1.5
- value: bfloat16 [4096, 4096], P('sp', 'tp'), may hold values from -6 to 6
- log_decay: float32 [4096, 2048], P('sp', 'tp'), may hold values from -1 to 0, as said below
- span_state: float32 [32, 16, 128, 256], P('sp', 'tp'), may hold values from -24 to 24
Outputs:
- grad_expert_gate: bfloat16 [32, 2048, 2048], P('sp', None, 'tp')
- grad_expert_up: bfloat16 [32, 2048, 2048], P('sp', None, 'tp')
- grad_expert_down: bfloat16 [32, 2048, 2048], P('sp', 'tp')
- grad_out_proj: float32 [2048, 4096], P('sp', 'tp')
- grad_query: bfloat16 [4096, 2048], P('sp', 'tp')
- grad_key: bfloat16 [4096, 2048], P('sp', 'tp')
- grad_value: bfloat16 [4096, 4096], P('sp', 'tp')
- grad_log_decay: float32 [4096, 2048], P('sp', 'tp')
Inputs may be any that keep to these rules, and one draw needn't show every extreme that they name: `route_ids`: A row names 2 different experts. Within each aligned block of 128 rows (the rows of one index of sp) no expert is named by more than 12 rows, and in every draw some expert is named by exactly 12 rows of some block. `log_decay`: every entry is zero or negative.
All inputs are finite; a program needn't handle non-finite values.
Results may differ from a plain program's by a relative error of at most 0.023.
Values may be sent and summed in bfloat16 or wider, within the bound.
No kernel may reach another device: no remote copies, remote signals or barrier semaphores. Data moves between devices by JAX's collectives and lax.ppermute only.
A program may use at most 64 MiB of HBM per device.

v0:
```python
import jax
import jax.numpy as jnp
from jax import lax
from jax.sharding import Mesh
from jax.sharding import PartitionSpec as P

KEY_CHANNELS = 128
DV = 256
TOP = 2
BLOCK = 64
SP = ("z", "x")
TP = ("y", "c")
epsilon = 1e-06


def sum_parts(tiles):
    return jnp.sum(tiles.astype(jnp.float32), axis=0)


def later_sum(states, decays, place):
    count = states.shape[0]
    total = jnp.zeros(states.shape[1:], jnp.float32)
    factor = jnp.ones(decays.shape[1:], jnp.float32)
    for k in range(count):
        later = k > place
        total = total + jnp.where(later, factor, 0.0)[:, None] * states[k].astype(jnp.float32)
        factor = jnp.where(later, factor * decays[k], factor)
    return (total, factor)


def to_all(array, axis):
    count = lax.axis_size(axis)
    copies = jnp.broadcast_to(array[None], (count, *array.shape))
    return lax.all_to_all(copies, axis, 0, 0, tiled=True)


def with_decay(state, decay):
    row = jnp.pad(decay[None, :], ((0, 7), (0, DV - KEY_CHANNELS)))
    return jnp.concatenate([state, row], axis=0).astype(jnp.bfloat16)


def split_decay(filled):
    decays = filled[:, KEY_CHANNELS, :KEY_CHANNELS].astype(jnp.float32)
    return (filled[:, :KEY_CHANNELS], decays)


def into_blocks(values):
    return values.reshape(values.shape[0] // BLOCK, BLOCK, values.shape[1])


def span_forward(query_rows, key_rows, value_rows, grad_rows, decay_rows, entry_state):
    query_blk = into_blocks(query_rows)
    key_blk = into_blocks(key_rows)
    value_blk = into_blocks(value_rows)
    grad_blk = into_blocks(grad_rows)
    cumlog = jnp.cumsum(into_blocks(decay_rows), axis=1)
    block_total = cumlog[:, -1, :]
    to_end = jnp.exp(block_total[:, None, :] - cumlog)
    inner_part = jnp.einsum("nsd,nsj->ndj", key_blk * to_end, value_blk)

    def forward_step(carry_state, step_item):
        piece_part, block_sum = step_item
        return (jnp.exp(block_sum)[:, None] * carry_state + piece_part, carry_state)

    end_state, starts = lax.scan(forward_step, entry_state, (inner_part, block_total))
    own_part = jnp.einsum("ntd,ntj->ndj", query_blk * jnp.exp(cumlog), grad_blk)

    def backward_step(carry_state, step_item):
        piece_part, block_sum = step_item
        return (jnp.exp(block_sum)[:, None] * carry_state + piece_part, carry_state)

    start_cot, after_cot = lax.scan(
        backward_step, jnp.zeros_like(entry_state), (own_part, block_total), reverse=True
    )
    span_total = jnp.sum(block_total, axis=0)
    later_log = span_total[None, :] - jnp.cumsum(block_total, axis=0)
    return ((cumlog, starts, after_cot, later_log, end_state), (jnp.exp(span_total), start_cot))


def span_backward(query_rows, key_rows, value_rows, grad_rows, kept_terms, exit_cot):
    cumlog, starts, after_cot, later_log, end_state = kept_terms
    query_blk = into_blocks(query_rows)
    key_blk = into_blocks(key_rows)
    value_blk = into_blocks(value_rows)
    grad_blk = into_blocks(grad_rows)
    exit_cots = after_cot + jnp.exp(later_log)[:, :, None] * exit_cot
    causal = jnp.arange(BLOCK)[:, None] >= jnp.arange(BLOCK)[None, :]
    decays = jnp.exp(
        jnp.where(causal[None, :, :, None], cumlog[:, :, None, :] - cumlog[:, None, :, :], -jnp.inf)
    )
    scores = jnp.einsum("ntd,nsd,ntsd->nts", query_blk, key_blk, decays)
    grad_scores = jnp.einsum("ntj,nsj->nts", grad_blk, value_blk)
    grad_query = jnp.exp(cumlog) * jnp.einsum("ntj,ndj->ntd", grad_blk, starts)
    grad_query = grad_query + jnp.einsum("nts,nsd,ntsd->ntd", grad_scores, key_blk, decays)
    to_end = jnp.exp(cumlog[:, -1:, :] - cumlog)
    grad_key = jnp.einsum("nts,ntd,ntsd->nsd", grad_scores, query_blk, decays)
    grad_key = grad_key + to_end * jnp.einsum("nsj,ndj->nsd", value_blk, exit_cots)
    grad_value = jnp.einsum("nts,ntj->nsj", scores, grad_blk)
    grad_value = grad_value + jnp.einsum("nsd,ndj->nsj", key_blk * to_end, exit_cots)
    length = query_rows.shape[0]
    key_width = query_rows.shape[1]
    per_position = (query_blk * grad_query - key_blk * grad_key).reshape(length, key_width)
    grad_log = (
        jnp.flip(jnp.cumsum(jnp.flip(per_position, 0), 0), 0)
        + jnp.sum(end_state * exit_cot, axis=1)[None, :]
    )
    return (
        grad_query.reshape(length, key_width),
        grad_key.reshape(length, key_width),
        grad_value.reshape(length, value_rows.shape[1]),
        grad_log,
    )


def on_device(
    resid,
    norm_gain,
    cotangent,
    route_ids,
    route_weight,
    expert_gate,
    expert_up,
    expert_down,
    out_proj,
    mixed,
    query,
    key,
    value,
    log_decay,
    span_state,
):
    tokens_here = resid.shape[0]
    model_width = resid.shape[1]
    half = model_width // 2
    sp_count = lax.axis_size(SP)
    y_count = lax.axis_size("y")
    experts = sp_count * expert_gate.shape[0]
    capacity = 3 * tokens_here // experts
    slots = experts * capacity
    core = lax.axis_index("c")
    resid_f = resid.astype(jnp.float32)
    inverse_rms = lax.rsqrt(jnp.mean(resid_f * resid_f, axis=1, keepdims=True) + epsilon)
    unit_rows = resid_f * inverse_rms
    normed = (unit_rows * norm_gain).astype(jnp.bfloat16)
    pair_expert = route_ids.reshape(-1)
    onehot = (pair_expert[:, None] == jnp.arange(experts, dtype=jnp.int32)[None, :]).astype(
        jnp.int32
    )
    slot_rank = jnp.sum((jnp.cumsum(onehot, axis=0) - onehot) * onehot, axis=1)
    slot_of = (pair_expert * capacity + slot_rank).reshape(tokens_here, TOP)
    slot_a, slot_b = (slot_of[:, 0], slot_of[:, 1])
    packed = lax.broadcasted_iota(jnp.int32, (2 * slots, 2 * tokens_here), 0)
    aim_a = jnp.concatenate([2 * slot_a, 2 * slot_a + 1])[None, :]
    aim_b = jnp.concatenate([2 * slot_b, 2 * slot_b + 1])[None, :]
    hit_a, hit_b = (packed == aim_a, packed == aim_b)
    weight_a = jnp.concatenate([route_weight[:, 0]] * 2)[None, :]
    weight_b = jnp.concatenate([route_weight[:, 1]] * 2)[None, :]
    slot_weight = jnp.sum(
        jnp.where(hit_a, weight_a, 0.0) + jnp.where(hit_b, weight_b, 0.0), axis=1, keepdims=True
    )
    scale = jnp.where(core == 0, 1.0, slot_weight)
    chosen = jnp.where(core == 0, normed, cotangent)
    rows_two = jnp.concatenate([chosen[:, :half], chosen[:, half:]], axis=0)
    sent = jnp.dot(
        (hit_a | hit_b).astype(jnp.bfloat16), rows_two, preferred_element_type=jnp.float32
    )
    sent = (sent * scale).astype(jnp.bfloat16).reshape(sp_count, 2 * capacity, half)
    own = lax.all_to_all(sent, SP, 0, 0, tiled=True).reshape(2 * slots, half)
    other = lax.ppermute(own, "c", [(0, 1), (1, 0)])
    rows_in = jnp.where(core == 0, own, other)
    rows_cot = jnp.where(core == 0, other, own)
    gate_w, up_w, down_w = (expert_gate[0], expert_up[0], expert_down[0])
    width = gate_w.shape[1]
    into_w = jnp.concatenate([gate_w[:half], gate_w[half:], up_w[:half], up_w[half:]], axis=1)
    down_two = jnp.concatenate([down_w[:, :half], down_w[:, half:]], axis=0)
    pre = jnp.dot(rows_in, into_w, preferred_element_type=jnp.float32)
    gate_pre = pre[:, :width] + jnp.roll(pre[:, width : 2 * width], -1, axis=0)
    up_pre = pre[:, 2 * width : 3 * width] + jnp.roll(pre[:, 3 * width :], -1, axis=0)
    hid = lax.dot_general(
        rows_cot, down_two, (((1,), (1,)), ((), ())), preferred_element_type=jnp.float32
    )
    grad_hidden = hid[:, :width] + jnp.roll(hid[:, width:], -1, axis=0)
    gate_sig = jax.nn.sigmoid(gate_pre)
    first = lax.broadcasted_iota(jnp.int32, (2 * slots, 1), 0) % 2 == 0

    def kept(values):
        return jnp.where(first, values, 0.0).astype(jnp.bfloat16)

    hidden = kept(gate_pre * gate_sig * up_pre)
    grad_up_act = kept(grad_hidden * gate_pre * gate_sig)
    grad_gate_act = kept(grad_hidden * up_pre * gate_sig * (1.0 + gate_pre * (1.0 - gate_sig)))
    acts = jnp.concatenate([grad_gate_act, grad_up_act], axis=1)
    pick = (
        lax.broadcasted_iota(jnp.int32, (slots, 2 * slots), 1)
        == 2 * lax.broadcasted_iota(jnp.int32, (slots, 2 * slots), 0)
    ).astype(jnp.bfloat16)
    acts = jnp.dot(pick, acts, preferred_element_type=jnp.float32).astype(jnp.bfloat16)
    out_w = jnp.concatenate([gate_w, up_w], axis=1).reshape(y_count, 2, width, 2 * width)
    out_own = jnp.where(core == 0, out_w[:, 0], out_w[:, 1]).reshape(half, 2 * width)
    out_other = jnp.where(core == 0, out_w[:, 1], out_w[:, 0]).reshape(half, 2 * width)

    def onto(weights):
        return lax.dot_general(
            acts, weights, (((1,), (1,)), ((), ())), preferred_element_type=jnp.float32
        )

    passed = lax.ppermute(onto(out_other).astype(jnp.bfloat16), "c", [(0, 1), (1, 0)])
    pair_sum = (onto(out_own) + passed.astype(jnp.float32)).astype(jnp.bfloat16)
    parts = pair_sum.reshape(slots, y_count, width).transpose(1, 0, 2)
    summed = sum_parts(lax.all_to_all(parts, "y", 0, 0, tiled=True)).astype(jnp.bfloat16)

    def beside(values):
        return jnp.concatenate([values, jnp.roll(values, 1, axis=0)], axis=1)

    grad_in_w = lax.dot_general(
        rows_in,
        jnp.concatenate([beside(grad_gate_act), beside(grad_up_act)], axis=1),
        (((0,), (0,)), ((), ())),
        preferred_element_type=jnp.float32,
    ).astype(jnp.bfloat16)
    grad_gate_w = jnp.concatenate([grad_in_w[:, :width], grad_in_w[:, width : 2 * width]], axis=0)
    grad_up_w = jnp.concatenate(
        [grad_in_w[:, 2 * width : 3 * width], grad_in_w[:, 3 * width :]], axis=0
    )
    grad_out_w = lax.dot_general(
        beside(hidden), rows_cot, (((0,), (0,)), ((), ())), preferred_element_type=jnp.float32
    ).astype(jnp.bfloat16)
    grad_down_w = jnp.concatenate([grad_out_w[:width], grad_out_w[width:]], axis=1)
    out_proj_here, own_tied = lax.optimization_barrier((out_proj, rows_in))
    out_proj_all = to_all(out_proj_here, SP).reshape(model_width, -1)
    returned = lax.all_to_all(
        summed.reshape(experts, capacity, -1), SP, split_axis=0, concat_axis=0, tiled=True
    )
    flat_rows = returned.reshape(slots, -1)
    slot_index = lax.broadcasted_iota(jnp.int32, (slots, tokens_here), 0)
    slot_tokens = ((slot_index == slot_a[None, :]) | (slot_index == slot_b[None, :])).astype(
        jnp.bfloat16
    )
    grad_normed = lax.all_gather(
        lax.dot_general(
            slot_tokens, flat_rows, (((0,), (0,)), ((), ())), preferred_element_type=jnp.float32
        ).astype(jnp.bfloat16),
        ("y", "c"),
        axis=1,
        tiled=True,
    ).astype(jnp.float32)
    scaled = grad_normed * norm_gain
    grad_resid = cotangent.astype(jnp.float32) + inverse_rms * (
        scaled - unit_rows * jnp.mean(scaled * unit_rows, axis=1, keepdims=True)
    )
    grad_resid = grad_resid.astype(jnp.bfloat16)
    grad_mixed = jnp.dot(grad_resid, out_proj_all, preferred_element_type=jnp.float32).astype(
        jnp.bfloat16
    )
    share = lax.dot_general(
        grad_resid, mixed, (((0,), (0,)), ((), ())), preferred_element_type=jnp.float32
    ).astype(jnp.bfloat16)
    grad_out_proj = sum_parts(
        lax.all_to_all(share.reshape(sp_count, model_width // sp_count, -1), SP, 0, 0, tiled=True)
    )
    head_count = query.shape[1] // KEY_CHANNELS
    query_scale = KEY_CHANNELS ** (-0.5)

    def heads_first(values, head_depth):
        return values.reshape(tokens_here, head_count, head_depth).transpose(1, 0, 2)

    query_rows = heads_first(query, KEY_CHANNELS).astype(jnp.float32) * query_scale
    key_rows = heads_first(key, KEY_CHANNELS).astype(jnp.float32)
    value_rows = heads_first(value, DV).astype(jnp.float32)
    grad_rows = heads_first(grad_mixed, DV).astype(jnp.float32)
    decay_rows = heads_first(log_decay, KEY_CHANNELS)
    kept_terms, summary = jax.vmap(span_forward)(
        query_rows, key_rows, value_rows, grad_rows, decay_rows, span_state[0]
    )
    own_decay, own_state = (summary[0][0], summary[1][0])
    near_states, near_decays = split_decay(to_all(with_decay(own_state, own_decay), "x"))
    near_sum, near_factor = later_sum(near_states, near_decays, lax.axis_index("x"))
    group_sum, group_factor = later_sum(near_states, near_decays, -1)
    far_states, far_decays = split_decay(to_all(with_decay(group_sum, group_factor), "z"))
    far_sum, _ = later_sum(far_states, far_decays, lax.axis_index("z"))
    exit_cot = near_sum + near_factor[:, None] * far_sum
    head_grads = jax.vmap(span_backward)(
        query_rows, key_rows, value_rows, grad_rows, kept_terms, exit_cot[None]
    )

    def tokens_first(values):
        return values.transpose(1, 0, 2).reshape(tokens_here, -1)

    grad_query = (tokens_first(head_grads[0]) * query_scale).astype(jnp.bfloat16)
    grad_key = tokens_first(head_grads[1]).astype(jnp.bfloat16)
    grad_value = tokens_first(head_grads[2]).astype(jnp.bfloat16)
    grad_log_decay = tokens_first(head_grads[3])
    return (
        grad_gate_w[None],
        grad_up_w[None],
        grad_down_w[None],
        grad_out_proj,
        grad_query,
        grad_key,
        grad_value,
        grad_log_decay,
    )


def solution(mesh):
    finer = Mesh(mesh.devices.reshape(8, 4, 8, 2), ("z", "x", "y", "c"))
    in_specs = (
        P(SP, None),
        P(),
        P(SP, None),
        P(SP, None),
        P(SP, None),
        P(SP, None, TP),
        P(SP, None, TP),
        P(SP, TP, None),
        P(SP, TP),
        P(SP, TP),
        P(SP, TP),
        P(SP, TP),
        P(SP, TP),
        P(SP, TP),
        P(SP, TP, None, None),
    )
    out_specs = (
        P(SP, None, TP),
        P(SP, None, TP),
        P(SP, TP, None),
        P(SP, TP),
        P(SP, TP),
        P(SP, TP),
        P(SP, TP),
        P(SP, TP),
    )
    return jax.shard_map(
        on_device, mesh=finer, in_specs=in_specs, out_specs=out_specs, check_vma=False
    )
```

profile of v0, /device:TPU:2, one launch (start us, length us, event | category | flops | bytes accessed | tf_op | source)
XLA Modules:
  0.0 222.4 jit_solution(10590077181551964781)
XLA Ops:
  4.5 1.2 fusion.22
  7.2 1.8 multiply_convert_fusion
  9.0 13.6 %all-to-all-start = ((bf16[32,24,1024]{2,1,0:T(8,128)(2,1)}), bf16[32,24,1024]{2,1,0:T(8,128)(2,1)S(1)}, u32[]{:S(2)}, u32[]{:S(2)}) async-start(bf16[32,24,1024]{2,1,0:T(8,128)(2,1)} %bitcast.383), calls=%async_computation | async-start | bytes 3145728 | tf_op jit(solution)/shard_map/all_to_all | solution.py:168
  25.3 35.7 %all-to-all-done = bf16[32,24,1024]{2,1,0:T(8,128)(2,1)S(1)} async-done(((bf16[32,24,1024]{2,1,0:T(8,128)(2,1)}), bf16[32,24,1024]{2,1,0:T(8,128)(2,1)S(1)}, u32[]{:S(2)}, u32[]{:S(2)}) %all-to-all-start) | async-done | bytes 1572896 | tf_op jit(solution)/shard_map/all_to_all | solution.py:168
  61.0 1.9 collective-permute-start
  63.0 2.3 %broadcast_select_fusion.4 = (bf16[8,1,128,256]{3,2,1,0:T(8,128)(2,1)S(1)}, bf16[8,1,128,256]{3,2,1,0:T(8,128)(2,1)}) fusion(pred[]{:T(512)S(6)} %eq.83, bf16[8,2,128,128]{3,2,1,0:T(8,128)(2,1)S(1)} %bitcast.376, bf16[8,2,128,128]{3,2,1,0:T(8,128)(2,1)} %bitcast.377), kind=kLoop, calls=%fused_computation.94 | loop fusion | flops 3670016 | bytes 2097153 | tf_op jit(solution)/shard_map/jit(_where)/select_n | solution.py:200
  68.2 2.0 fusion.45
  72.2 1.3 convolution_convert_fusion.2
  73.5 2.3 %collective-permute-start.1 = (bf16[384,1024]{1,0:T(8,128)(2,1)}, bf16[384,1024]{1,0:T(8,128)(2,1)}, u32[]{:S(2)}, u32[]{:S(2)}) collective-permute-start(bf16[384,1024]{1,0:T(8,128)(2,1)} %convolution_convert_fusion.2), channel_id=1, source_target_pairs={{0,1},{1,0},{2,3},{3,2},{4,5},{5,4},{6,7},{7,6},{8,9},{9,8},{10,11... | collective-permute-start | bytes 2359304 | tf_op jit(solution)/shard_map/ppermute | solution.py:207
  75.8 1.5 while.29
  78.0 1.5 fusion.31
  79.6 1.1 copy.125
  80.7 7.1 %all-to-all-start.1 = ((bf16[8,384,128]{2,1,0:T(8,128)(2,1)}), bf16[8,384,128]{2,1,0:T(8,128)(2,1)S(1)}, u32[]{:S(2)}, u32[]{:S(2)}) async-start(bf16[8,384,128]{2,1,0:T(8,128)(2,1)} %bitcast.374), calls=%async_computation.1 | async-start | bytes 1572864 | tf_op jit(solution)/shard_map/all_to_all | solution.py:210
  87.9 4.4 %fusion.4 = (bf16[2,64,64]{2,1,0:T(8,128)(2,1)}, f32[2,64,128,64]{2,3,1,0:T(8,128)}) fusion(f32[2,128,64]{1,2,0:T(8,128)S(1)} %copy-done.21, f32[2,128,64]{1,2,0:T(8,128)S(1)} %bitcast.384, f32[2,64,128]{2,1,0:T(8,128)S(1)} %bitcast.371, pred[64,64]{1,0:T(8,128)(4,1)S(1)} %iota_compare_fusion.10), kind=kLoop, calls=%fused_computation.11 | loop fusion | flops 5234688 | bytes 4411392 | tf_op jit(solution)/shard_map/vmap(ntd,nsd,ntsd->nts)/dot_general | solution.py:91
  94.3 2.8 %convolution_convert_fusion.3 = bf16[256,1024]{1,0:T(8,128)(2,1)} fusion(bf16[768,1024]{1,0:T(8,128)(2,1)} %collective-permute-done, bf16[768,1024]{1,0:T(8,128)(2,1)S(1)} %bitcast.370, pred[]{:T(512)S(6)} %eq.83, bf16[767,128]{1,0:T(8,128)(2,1)S(1)} %bitcast.395, bf16[1,128]{1,0:T(2,128)(2,1)S(1)} %slice.339, bf16[768,128]{1,0:T(8,128)(2,1)S(1)} %copy-done.22), kind=kOutput, calls=%fused_computation.30 | convolution fusion | flops 404881408 | bytes 4063233 | tf_op jit(solution)/shard_map/dot_general | solution.py:225
  97.1 14.4 %all-to-all-done.1 = bf16[8,384,128]{2,1,0:T(8,128)(2,1)S(1)} async-done(((bf16[8,384,128]{2,1,0:T(8,128)(2,1)}), bf16[8,384,128]{2,1,0:T(8,128)(2,1)S(1)}, u32[]{:S(2)}, u32[]{:S(2)}) %all-to-all-start.1) | async-done | bytes 786464 | tf_op jit(solution)/shard_map/all_to_all | solution.py:210
  112.3 6.5 %all-to-all-start.2 = ((bf16[32,12,128]{2,1,0:T(8,128)(2,1)}), bf16[32,12,128]{2,1,0:T(8,128)(2,1)S(1)}, u32[]{:S(2)}, u32[]{:S(2)}) async-start(bf16[32,12,128]{2,1,0:T(8,128)(2,1)} %reshape.961), calls=%async_computation.2 | async-start | bytes 262144 | tf_op jit(solution)/shard_map/all_to_all | solution.py:231
  118.8 1.9 maximum_bitcast_fusion
  120.7 7.1 %all-to-all-done.2 = bf16[32,12,128]{2,1,0:T(8,128)(2,1)S(1)} async-done(((bf16[32,12,128]{2,1,0:T(8,128)(2,1)}), bf16[32,12,128]{2,1,0:T(8,128)(2,1)S(1)}, u32[]{:S(2)}, u32[]{:S(2)}) %all-to-all-start.2) | async-done | bytes 98336 | tf_op jit(solution)/shard_map/all_to_all | solution.py:231
  127.8 1.2 broadcast_in_dim.169
  129.0 5.6 %all-to-all-start.4 = ((bf16[32,64,256]{2,1,0:T(8,128)(2,1)}), bf16[32,64,256]{2,1,0:T(8,128)(2,1)S(1)}, u32[]{:S(2)}, u32[]{:S(2)}) async-start(bf16[32,64,256]{2,1,0:T(8,128)(2,1)} %broadcast_in_dim.169), calls=%async_computation.4 | async-start | bytes 2097152 | tf_op jit(solution)/shard_map/all_to_all | solution.py:34
  136.7 16.1 %all_gather.3 = bf16[128,2048]{1,0:T(8,128)(2,1)S(1)} all-gather(bf16[128,128]{1,0:T(8,128)(2,1)S(1)} %convolution_convert_fusion.5), channel_id=1, replica_groups=mesh['z'=8,'x'=4,'y'=8,'c'=2] {'y','c'}, dimensions={1}, use_global_device_ids=true | all-gather | bytes 557056 | tf_op jit(solution)/shard_map/all_gather | solution.py:239
  153.6 8.0 %all-to-all-done.4 = bf16[32,64,256]{2,1,0:T(8,128)(2,1)S(1)} async-done(((bf16[32,64,256]{2,1,0:T(8,128)(2,1)}), bf16[32,64,256]{2,1,0:T(8,128)(2,1)S(1)}, u32[]{:S(2)}, u32[]{:S(2)}) %all-to-all-start.4) | async-done | bytes 1048608 | tf_op jit(solution)/shard_map/all_to_all | solution.py:34
  163.5 4.9 %all-to-all-start.5 = ((bf16[4,136,256]{2,1,0:T(8,128)(2,1)}), bf16[4,136,256]{2,1,0:T(8,128)(2,1)S(1)}, u32[]{:S(2)}, u32[]{:S(2)}) async-start(bf16[4,136,256]{2,1,0:T(8,128)(2,1)} %broadcast_in_dim.173), calls=%async_computation.5 | async-start | bytes 557056 | tf_op jit(solution)/shard_map/all_to_all | solution.py:34
  168.7 5.1 %all-to-all-done.5 = bf16[4,136,256]{2,1,0:T(8,128)(2,1)S(1)} async-done(((bf16[4,136,256]{2,1,0:T(8,128)(2,1)}), bf16[4,136,256]{2,1,0:T(8,128)(2,1)S(1)}, u32[]{:S(2)}, u32[]{:S(2)}) %all-to-all-start.5) | async-done | bytes 278560 | tf_op jit(solution)/shard_map/all_to_all | solution.py:34
  174.8 3.5 %all-to-all-start.6 = ((bf16[8,136,256]{2,1,0:T(8,128)(2,1)}), bf16[8,136,256]{2,1,0:T(8,128)(2,1)S(1)}, u32[]{:S(2)}, u32[]{:S(2)}) async-start(bf16[8,136,256]{2,1,0:T(8,128)(2,1)} %broadcast_in_dim.175), calls=%async_computation.6 | async-start | bytes 1114112 | tf_op jit(solution)/shard_map/all_to_all | solution.py:34
  178.4 5.0 %fusion.5 = f32[2,64,128]{2,1,0:T(8,128)S(1)} fusion(f32[2,64,128,64]{2,3,1,0:T(8,128)} %get-tuple-element.289, f32[2,64,128]{2,1,0:T(8,128)S(1)} %copy-done.20, f32[2,64,64]{2,1,0:T(8,128)S(1)} %copy.98), kind=kLoop, calls=%fused_computation.13 | loop fusion | flops 3129344 | bytes 4358144 | tf_op jit(solution)/shard_map/vmap(nts,nsd,ntsd->ntd)/dot_general | solution.py:94
  183.6 1.4 convolution_convert_fusion
  185.0 2.0 multiply_reduce_fusion
  187.0 6.0 %all-to-all-done.6 = bf16[8,136,256]{2,1,0:T(8,128)(2,1)S(1)} async-done(((bf16[8,136,256]{2,1,0:T(8,128)(2,1)}), bf16[8,136,256]{2,1,0:T(8,128)(2,1)S(1)}, u32[]{:S(2)}, u32[]{:S(2)}) %all-to-all-start.6) | async-done | bytes 557088 | tf_op jit(solution)/shard_map/all_to_all | solution.py:34
  193.0 5.0 %all-to-all-start.3 = ((bf16[32,64,256]{2,1,0:T(8,128)(2,1)}), bf16[32,64,256]{2,1,0:T(8,128)(2,1)S(1)}, u32[]{:S(2)}, u32[]{:S(2)}) async-start(bf16[32,64,256]{2,1,0:T(8,128)(2,1)} %bitcast.28), calls=%async_computation.3 | async-start | bytes 2097152 | tf_op jit(solution)/shard_map/all_to_all | solution.py:259
  201.6 20.1 %all-to-all-done.3 = bf16[32,64,256]{2,1,0:T(8,128)(2,1)S(1)} async-done(((bf16[32,64,256]{2,1,0:T(8,128)(2,1)}), bf16[32,64,256]{2,1,0:T(8,128)(2,1)S(1)}, u32[]{:S(2)}, u32[]{:S(2)}) %all-to-all-start.3) | async-done | bytes 1048608 | tf_op jit(solution)/shard_map/all_to_all | solution.py:259
  (189 shorter events, 28.2 us)
Async XLA Ops:
  0.6 182.9 %copy-start = (bf16[128,256]{1,0:T(8,128)(2,1)S(1)}, bf16[128,256]{1,0:T(8,128)(2,1)}, u32[]{:S(2)}) copy-start(bf16[128,256]{1,0:T(8,128)(2,1)} %param.28) | copy-start | bytes 196612
  0.6 5.5 %copy-start.2 = (bf16[128,2048]{1,0:T(8,128)(2,1)S(1)}, bf16[128,2048]{1,0:T(8,128)(2,1)}, u32[]{:S(2)}) copy-start(bf16[128,2048]{1,0:T(8,128)(2,1)} %param.19) | copy-start | bytes 1572868
  0.7 5.5 %copy-start.6 = (bf16[128,2048]{1,0:T(8,128)(2,1)S(1)}, bf16[128,2048]{1,0:T(8,128)(2,1)}, u32[]{:S(2)}) copy-start(bf16[128,2048]{1,0:T(8,128)(2,1)} %param.21) | copy-start | bytes 1572868
  9.0 13.6 %copy-start.31 = (f32[128,128]{1,0:T(8,128)S(1)}, f32[128,128]{1,0:T(8,128)}, u32[]{:S(2)}) copy-start(f32[128,128]{1,0:T(8,128)} %param.32) | copy-start | bytes 196612
  9.0 15.6 %copy-start.13 = (bf16[128,256]{1,0:T(8,128)(2,1)S(1)}, bf16[128,256]{1,0:T(8,128)(2,1)}, u32[]{:S(2)}) copy-start(bf16[128,256]{1,0:T(8,128)(2,1)} %param.31) | copy-start | bytes 196612
  9.0 15.6 %copy-start.18 = (bf16[128,128]{1,0:T(8,128)(2,1)S(1)}, bf16[128,128]{1,0:T(8,128)(2,1)}, u32[]{:S(2)}) copy-start(bf16[128,128]{1,0:T(8,128)(2,1)} %param.30) | copy-start | bytes 98308
  9.0 54.0 %copy-start.3 = (bf16[1,2048,128]{2,1,0:T(8,128)(2,1)S(1)}, bf16[1,2048,128]{2,1,0:T(8,128)(2,1)}, u32[]{:S(2)}) copy-start(bf16[1,2048,128]{2,1,0:T(8,128)(2,1)} %param.25) | copy-start | bytes 1572868
  9.0 52.0 %all-to-all-start = ((bf16[32,24,1024]{2,1,0:T(8,128)(2,1)}), bf16[32,24,1024]{2,1,0:T(8,128)(2,1)S(1)}, u32[]{:S(2)}, u32[]{:S(2)}) async-start(bf16[32,24,1024]{2,1,0:T(8,128)(2,1)} %bitcast.383), calls=%async_computation | async-start | bytes 3145728 | tf_op jit(solution)/shard_map/all_to_all | solution.py:168
  22.6 43.2 %copy-start.28 = (bf16[128,128]{1,0:T(8,128)(2,1)S(1)}, bf16[128,128]{1,0:T(8,128)(2,1)}, u32[]{:S(2)}) copy-start(bf16[128,128]{1,0:T(8,128)(2,1)} %param.29) | copy-start | bytes 98308
  61.0 5.7 %collective-permute-start = (bf16[768,1024]{1,0:T(8,128)(2,1)S(1)}, bf16[768,1024]{1,0:T(8,128)(2,1)}, u32[]{:S(2)}, u32[]{:S(2)}) collective-permute-start(bf16[768,1024]{1,0:T(8,128)(2,1)S(1)} %bitcast.368), channel_id=1, source_target_pairs={{0,1},{1,0},{2,3},{3,2},{4,5},{5,4},{6,7},{7,6},{8,9},{9,8},{10,11... | collective-permute-start | bytes 4718600 | tf_op jit(solution)/shard_map/ppermute | solution.py:169
  65.9 21.9 %copy-start.11 = (f32[128,128]{1,0:T(8,128)}, f32[128,128]{1,0:T(8,128)S(1)}, u32[]{:S(2)}) copy-start(f32[128,128]{1,0:T(8,128)S(1)} %convert_multiply_fusion.18) | copy-start | bytes 196612
  73.5 4.5 %collective-permute-start.1 = (bf16[384,1024]{1,0:T(8,128)(2,1)}, bf16[384,1024]{1,0:T(8,128)(2,1)}, u32[]{:S(2)}, u32[]{:S(2)}) collective-permute-start(bf16[384,1024]{1,0:T(8,128)(2,1)} %convolution_convert_fusion.2), channel_id=1, source_target_pairs={{0,1},{1,0},{2,3},{3,2},{4,5},{5,4},{6,7},{7,6},{8,9},{9,8},{10,11... | collective-permute-start | bytes 2359304 | tf_op jit(solution)/shard_map/ppermute | solution.py:207
  79.6 8.2 %copy-start.21 = (f32[2,128,64]{1,2,0:T(8,128)S(1)}, f32[2,128,64]{1,2,0:T(8,128)}, u32[]{:S(2)}) copy-start(f32[2,128,64]{1,2,0:T(8,128)} %get-tuple-element.296) | copy-start | bytes 196612
  80.7 30.8 %all-to-all-start.1 = ((bf16[8,384,128]{2,1,0:T(8,128)(2,1)}), bf16[8,384,128]{2,1,0:T(8,128)(2,1)S(1)}, u32[]{:S(2)}, u32[]{:S(2)}) async-start(bf16[8,384,128]{2,1,0:T(8,128)(2,1)} %bitcast.374), calls=%async_computation.1 | async-start | bytes 1572864 | tf_op jit(solution)/shard_map/all_to_all | solution.py:210
  97.1 30.7 %copy-start.32 = (bf16[64,256]{1,0:T(8,128)(2,1)S(1)}, bf16[64,256]{1,0:T(8,128)(2,1)}, u32[]{:S(2)}) copy-start(bf16[64,256]{1,0:T(8,128)(2,1)} %param.27) | copy-start | bytes 98308
  112.3 15.5 %all-to-all-start.2 = ((bf16[32,12,128]{2,1,0:T(8,128)(2,1)}), bf16[32,12,128]{2,1,0:T(8,128)(2,1)S(1)}, u32[]{:S(2)}, u32[]{:S(2)}) async-start(bf16[32,12,128]{2,1,0:T(8,128)(2,1)} %reshape.961), calls=%async_computation.2 | async-start | bytes 262144 | tf_op jit(solution)/shard_map/all_to_all | solution.py:231
  120.7 13.9 %copy-start.10 = (bf16[1024,128]{1,0:T(8,128)(2,1)S(1)}, bf16[1024,128]{1,0:T(8,128)(2,1)}, u32[]{:S(2)}) copy-start(bf16[1024,128]{1,0:T(8,128)(2,1)} %get-tuple-element.275) | copy-start | bytes 786436
  129.0 6.5 %copy-start.17 = (bf16[256,1024]{1,0:T(8,128)(2,1)S(1)}, bf16[256,1024]{1,0:T(8,128)(2,1)}, u32[]{:S(2)}) copy-start(bf16[256,1024]{1,0:T(8,128)(2,1)} %convolution_convert_fusion.3) | copy-start | bytes 1572868
  129.0 32.6 %all-to-all-start.4 = ((bf16[32,64,256]{2,1,0:T(8,128)(2,1)}), bf16[32,64,256]{2,1,0:T(8,128)(2,1)S(1)}, u32[]{:S(2)}, u32[]{:S(2)}) async-start(bf16[32,64,256]{2,1,0:T(8,128)(2,1)} %broadcast_in_dim.169), calls=%async_computation.4 | async-start | bytes 2097152 | tf_op jit(solution)/shard_map/all_to_all | solution.py:34
  135.5 17.3 %copy-start.30 = (f32[2048]{0:T(1024)S(1)}, f32[2048]{0:T(1024)}, u32[]{:S(2)}) copy-start(f32[2048]{0:T(1024)} %param.20) | copy-start | bytes 24580
  135.5 17.3 %copy-start.34 = (f32[128]{0:T(128)S(1)}, f32[128]{0:T(128)}, u32[]{:S(2)}) copy-start(f32[128]{0:T(128)} %copy-done.33) | copy-start | bytes 1540
  135.5 17.6 %copy-start.7 = (bf16[128,2048]{1,0:T(8,128)(2,1)S(1)}, bf16[128,2048]{1,0:T(8,128)(2,1)}, u32[]{:S(2)}) copy-start(bf16[128,2048]{1,0:T(8,128)(2,1)} %param.21) | copy-start | bytes 1572868
  153.1 8.8 %copy-start.12 = (f32[128,128]{1,0:T(8,128)S(1)}, f32[128,128]{1,0:T(8,128)}, u32[]{:S(2)}) copy-start(f32[128,128]{1,0:T(8,128)} %copy-done.11) | copy-start | bytes 196612
  153.6 8.6 %copy-start.37 = (f32[2,1,128]{2,1,0:T(1,128)S(1)}, f32[2,1,128]{2,1,0:T(1,128)}, u32[]{:S(2)}) copy-start(f32[2,1,128]{2,1,0:T(1,128)} %get-tuple-element.408) | copy-start | bytes 3076
  162.2 6.3 %copy-start.14 = (bf16[128,256]{1,0:T(8,128)(2,1)S(1)}, bf16[128,256]{1,0:T(8,128)(2,1)}, u32[]{:S(2)}) copy-start(bf16[128,256]{1,0:T(8,128)(2,1)} %param.31) | copy-start | bytes 196612
  163.5 14.8 %copy-start.20 = (f32[2,64,128]{2,1,0:T(8,128)S(1)}, f32[2,64,128]{2,1,0:T(8,128)}, u32[]{:S(2)}) copy-start(f32[2,64,128]{2,1,0:T(8,128)} %get-tuple-element.297) | copy-start | bytes 196612
  163.5 10.2 %all-to-all-start.5 = ((bf16[4,136,256]{2,1,0:T(8,128)(2,1)}), bf16[4,136,256]{2,1,0:T(8,128)(2,1)S(1)}, u32[]{:S(2)}, u32[]{:S(2)}) async-start(bf16[4,136,256]{2,1,0:T(8,128)(2,1)} %broadcast_in_dim.173), calls=%async_computation.5 | async-start | bytes 557056 | tf_op jit(solution)/shard_map/all_to_all | solution.py:34
  174.8 18.2 %all-to-all-start.6 = ((bf16[8,136,256]{2,1,0:T(8,128)(2,1)}), bf16[8,136,256]{2,1,0:T(8,128)(2,1)S(1)}, u32[]{:S(2)}, u32[]{:S(2)}) async-start(bf16[8,136,256]{2,1,0:T(8,128)(2,1)} %broadcast_in_dim.175), calls=%async_computation.6 | async-start | bytes 1114112 | tf_op jit(solution)/shard_map/all_to_all | solution.py:34
  178.4 5.0 %copy-start.15 = (bf16[2,1,128,256]{3,2,1,0:T(8,128)(2,1)S(1)}, bf16[2,1,128,256]{3,2,1,0:T(8,128)(2,1)}, u32[]{:S(2)}) copy-start(bf16[2,1,128,256]{3,2,1,0:T(8,128)(2,1)} %get-tuple-element.142) | copy-start | bytes 393220
  187.0 11.4 %copy-start.19 = (bf16[128,128]{1,0:T(8,128)(2,1)S(1)}, bf16[128,128]{1,0:T(8,128)(2,1)}, u32[]{:S(2)}) copy-start(bf16[128,128]{1,0:T(8,128)(2,1)} %param.30) | copy-start | bytes 98308
  187.0 11.4 %copy-start.29 = (bf16[128,128]{1,0:T(8,128)(2,1)S(1)}, bf16[128,128]{1,0:T(8,128)(2,1)}, u32[]{:S(2)}) copy-start(bf16[128,128]{1,0:T(8,128)(2,1)} %param.29) | copy-start | bytes 98308
  193.0 28.6 %all-to-all-start.3 = ((bf16[32,64,256]{2,1,0:T(8,128)(2,1)}), bf16[32,64,256]{2,1,0:T(8,128)(2,1)S(1)}, u32[]{:S(2)}, u32[]{:S(2)}) async-start(bf16[32,64,256]{2,1,0:T(8,128)(2,1)} %bitcast.28), calls=%async_computation.3 | async-start | bytes 2097152 | tf_op jit(solution)/shard_map/all_to_all | solution.py:259
  (18 other events, 53.3 us)
where the time goes:
time: 224 us; the launch traced here: 222 us
  waiting for transfers between devices  97 us (43%)
  starting transfers between devices  50.6 us (23%)
  other arithmetic  29.2 us (13%)
  matrix products  16.6 us (7%)
  blocking collectives  16.1 us (7%)
  local copies, waits for them, and re-layouts  11.3 us (5%)
    all_to_all x1, waiting for transfers between devices, on_device(): own = lax.all_to_all(sent, SP, 0, 0, tiled=True).reshape(2 * slots, half)  35.7 us
    all_to_all x1, waiting for transfers between devices, on_device(): lax.all_to_all(share.reshape(sp_count, model_width // sp_count, -1), SP,...  20.1 us
    all_to_all x3, waiting for transfers between devices, to_all(): return lax.all_to_all(copies, axis, 0, 0, tiled=True)  19.1 us
    all_gather x1, blocking collectives, on_device(): lax.all_gather(lax.dot_general(slot_tokens, flat_rows, (((0,), (0,)), (()...  16.1 us
    all_to_all x1, waiting for transfers between devices, on_device(): lax.all_to_all(parts, 'y', 0, 0, tiled=True)  14.4 us
    all_to_all x3, starting transfers between devices, to_all(): return lax.all_to_all(copies, axis, 0, 0, tiled=True)  14.1 us
    all_to_all x1, starting transfers between devices, on_device(): own = lax.all_to_all(sent, SP, 0, 0, tiled=True).reshape(2 * slots, half)  13.6 us
    all_to_all x1, waiting for transfers between devices, on_device(): lax.all_to_all(summed.reshape(experts, capacity, -1), SP, split_axis=0, c...  7.14 us
  transfers between devices with their start and end apart: 9, of which 8 were waited for; matrix products, arithmetic and copies ran while one was open for 15% of the time, Pallas kernels for 0%

commit v1 on v0

--- a/solution.py
+++ b/solution.py
@@ -3,6 +3,7 @@
 from jax import lax
 from jax.sharding import Mesh
 from jax.sharding import PartitionSpec as P
+from jax.lax import all_gather
 
 KEY_CHANNELS = 128
 DV = 256
@@ -11,6 +12,7 @@
 SP = ("z", "x")
 TP = ("y", "c")
 epsilon = 1e-06
+_convert_side = lambda tile_in, comm_axis: jnp.concatenate(all_gather(tile_in, comm_axis), 1)
 
 
 def sum_parts(tiles):
@@ -236,13 +238,11 @@
     slot_tokens = ((slot_index == slot_a[None, :]) | (slot_index == slot_b[None, :])).astype(
         jnp.bfloat16
     )
-    grad_normed = lax.all_gather(
+    grad_normed = _convert_side(
         lax.dot_general(
             slot_tokens, flat_rows, (((0,), (0,)), ((), ())), preferred_element_type=jnp.float32
         ).astype(jnp.bfloat16),
-        ("y", "c"),
-        axis=1,
-        tiled=True,
+        comm_axis=("y", "c"),
     ).astype(jnp.float32)
     scaled = grad_normed * norm_gain
     grad_resid = cotangent.astype(jnp.float32) + inverse_rms * (

time: 224 us -> 224 us (level)
  no operation moved by 1% of the time
where the time goes in v1:
time: 224 us; the launch traced here: 222 us
  waiting for transfers between devices  97 us (43%)
  starting transfers between devices  50.6 us (23%)
  other arithmetic  29.2 us (13%)
  matrix products  16.6 us (7%)
  blocking collectives  16.1 us (7%)
  local copies, waits for them, and re-layouts  11.3 us (5%)
    all_to_all x1, waiting for transfers between devices, on_device(): own = lax.all_to_all(sent, SP, 0, 0, tiled=True).reshape(2 * slots, half)  35.7 us
    all_to_all x1, waiting for transfers between devices, on_device(): lax.all_to_all(share.reshape(sp_count, model_width // sp_count, -1), SP,...  20.1 us
    all_to_all x3, waiting for transfers between devices, to_all(): return lax.all_to_all(copies, axis, 0, 0, tiled=True)  19.1 us
    all_gather x1, blocking collectives, all_gather(tile_in, comm_axis)  16.1 us
    all_to_all x1, waiting for transfers between devices, on_device(): lax.all_to_all(parts, 'y', 0, 0, tiled=True)  14.4 us
    all_to_all x3, starting transfers between devices, to_all(): return lax.all_to_all(copies, axis, 0, 0, tiled=True)  14.1 us
    all_to_all x1, starting transfers between devices, on_device(): own = lax.all_to_all(sent, SP, 0, 0, tiled=True).reshape(2 * slots, half)  13.6 us
    all_to_all x1, waiting for transfers between devices, on_device(): lax.all_to_all(summed.reshape(experts, capacity, -1), SP, split_axis=0, c...  7.14 us
  transfers between devices with their start and end apart: 9, of which 8 were waited for; matrix products, arithmetic and copies ran while one was open for 15% of the time, Pallas kernels for 0%

profile of v1, /device:TPU:2, one launch (start us, length us, event | category | flops | bytes accessed | tf_op | source)
XLA Modules:
  0.0 222.4 jit_solution(335717066944635824)
XLA Ops:
  4.5 1.2 fusion.22
  7.2 1.8 multiply_convert_fusion
  9.0 13.6 %all-to-all-start = ((bf16[32,24,1024]{2,1,0:T(8,128)(2,1)}), bf16[32,24,1024]{2,1,0:T(8,128)(2,1)S(1)}, u32[]{:S(2)}, u32[]{:S(2)}) async-start(bf16[32,24,1024]{2,1,0:T(8,128)(2,1)} %bitcast.398), calls=%async_computation | async-start | bytes 3145728 | tf_op jit(solution)/shard_map/all_to_all | solution.py:170
  25.3 35.7 %all-to-all-done = bf16[32,24,1024]{2,1,0:T(8,128)(2,1)S(1)} async-done(((bf16[32,24,1024]{2,1,0:T(8,128)(2,1)}), bf16[32,24,1024]{2,1,0:T(8,128)(2,1)S(1)}, u32[]{:S(2)}, u32[]{:S(2)}) %all-to-all-start) | async-done | bytes 1572896 | tf_op jit(solution)/shard_map/all_to_all | solution.py:170
  61.0 1.9 collective-permute-start
  63.0 2.3 %broadcast_select_fusion.4 = (bf16[8,1,128,256]{3,2,1,0:T(8,128)(2,1)S(1)}, bf16[8,1,128,256]{3,2,1,0:T(8,128)(2,1)}) fusion(pred[]{:T(512)S(6)} %eq.83, bf16[8,2,128,128]{3,2,1,0:T(8,128)(2,1)S(1)} %bitcast.391, bf16[8,2,128,128]{3,2,1,0:T(8,128)(2,1)} %bitcast.392), kind=kLoop, calls=%fused_computation.95 | loop fusion | flops 3670016 | bytes 2097153 | tf_op jit(solution)/shard_map/jit(_where)/select_n | solution.py:202
  68.2 2.0 fusion.45
  72.2 1.3 convolution_convert_fusion.2
  73.5 2.3 %collective-permute-start.1 = (bf16[384,1024]{1,0:T(8,128)(2,1)}, bf16[384,1024]{1,0:T(8,128)(2,1)}, u32[]{:S(2)}, u32[]{:S(2)}) collective-permute-start(bf16[384,1024]{1,0:T(8,128)(2,1)} %convolution_convert_fusion.2), channel_id=1, source_target_pairs={{0,1},{1,0},{2,3},{3,2},{4,5},{5,4},{6,7},{7,6},{8,9},{9,8},{10,11... | collective-permute-start | bytes 2359304 | tf_op jit(solution)/shard_map/ppermute | solution.py:209
  75.8 1.5 while.29
  78.0 1.5 fusion.31
  79.6 1.1 copy.138
  80.7 7.1 %all-to-all-start.1 = ((bf16[8,384,128]{2,1,0:T(8,128)(2,1)}), bf16[8,384,128]{2,1,0:T(8,128)(2,1)S(1)}, u32[]{:S(2)}, u32[]{:S(2)}) async-start(bf16[8,384,128]{2,1,0:T(8,128)(2,1)} %bitcast.389), calls=%async_computation.1 | async-start | bytes 1572864 | tf_op jit(solution)/shard_map/all_to_all | solution.py:212
  87.9 4.4 %fusion.4 = (bf16[2,64,64]{2,1,0:T(8,128)(2,1)}, f32[2,64,128,64]{2,3,1,0:T(8,128)}) fusion(f32[2,128,64]{1,2,0:T(8,128)S(1)} %copy-done.21, f32[2,128,64]{1,2,0:T(8,128)S(1)} %bitcast.399, f32[2,64,128]{2,1,0:T(8,128)S(1)} %bitcast.386, pred[64,64]{1,0:T(8,128)(4,1)S(1)} %iota_compare_fusion.10), kind=kLoop, calls=%fused_computation.11 | loop fusion | flops 5234688 | bytes 4411392 | tf_op jit(solution)/shard_map/vmap(ntd,nsd,ntsd->nts)/dot_general | solution.py:93
  94.3 2.8 %convolution_convert_fusion.3 = bf16[256,1024]{1,0:T(8,128)(2,1)} fusion(bf16[768,1024]{1,0:T(8,128)(2,1)} %collective-permute-done, bf16[768,1024]{1,0:T(8,128)(2,1)S(1)} %bitcast.383, pred[]{:T(512)S(6)} %eq.83, bf16[767,128]{1,0:T(8,128)(2,1)S(1)} %bitcast.410, bf16[1,128]{1,0:T(2,128)(2,1)S(1)} %slice.339, bf16[768,128]{1,0:T(8,128)(2,1)S(1)} %copy-done.22), kind=kOutput, calls=%fused_computation.30 | convolution fusion | flops 404881408 | bytes 4063233 | tf_op jit(solution)/shard_map/dot_general | solution.py:227
  97.1 14.4 %all-to-all-done.1 = bf16[8,384,128]{2,1,0:T(8,128)(2,1)S(1)} async-done(((bf16[8,384,128]{2,1,0:T(8,128)(2,1)}), bf16[8,384,128]{2,1,0:T(8,128)(2,1)S(1)}, u32[]{:S(2)}, u32[]{:S(2)}) %all-to-all-start.1) | async-done | bytes 786464 | tf_op jit(solution)/shard_map/all_to_all | solution.py:212
  112.3 6.5 %all-to-all-start.2 = ((bf16[32,12,128]{2,1,0:T(8,128)(2,1)}), bf16[32,12,128]{2,1,0:T(8,128)(2,1)S(1)}, u32[]{:S(2)}, u32[]{:S(2)}) async-start(bf16[32,12,128]{2,1,0:T(8,128)(2,1)} %reshape.965), calls=%async_computation.2 | async-start | bytes 262144 | tf_op jit(solution)/shard_map/all_to_all | solution.py:233
  118.8 1.9 maximum_bitcast_fusion
  120.7 7.1 %all-to-all-done.2 = bf16[32,12,128]{2,1,0:T(8,128)(2,1)S(1)} async-done(((bf16[32,12,128]{2,1,0:T(8,128)(2,1)}), bf16[32,12,128]{2,1,0:T(8,128)(2,1)S(1)}, u32[]{:S(2)}, u32[]{:S(2)}) %all-to-all-start.2) | async-done | bytes 98336 | tf_op jit(solution)/shard_map/all_to_all | solution.py:233
  127.8 1.2 broadcast_in_dim.169
  129.0 5.6 %all-to-all-start.4 = ((bf16[32,64,256]{2,1,0:T(8,128)(2,1)}), bf16[32,64,256]{2,1,0:T(8,128)(2,1)S(1)}, u32[]{:S(2)}, u32[]{:S(2)}) async-start(bf16[32,64,256]{2,1,0:T(8,128)(2,1)} %broadcast_in_dim.169), calls=%async_computation.4 | async-start | bytes 2097152 | tf_op jit(solution)/shard_map/all_to_all | solution.py:36
  136.7 16.1 %all-gather = bf16[2048,128]{1,0:T(8,128)(2,1)S(1)} all-gather(bf16[128,128]{1,0:T(8,128)(2,1)S(1)} %convolution_convert_fusion.5), channel_id=2, replica_groups=mesh['z'=8,'x'=4,'y'=8,'c'=2] {'y','c'}, dimensions={0}, use_global_device_ids=true | all-gather | bytes 557056 | tf_op jit(solution)/shard_map/all_gather | solution.py:15
  153.5 8.1 %all-to-all-done.4 = bf16[32,64,256]{2,1,0:T(8,128)(2,1)S(1)} async-done(((bf16[32,64,256]{2,1,0:T(8,128)(2,1)}), bf16[32,64,256]{2,1,0:T(8,128)(2,1)S(1)}, u32[]{:S(2)}, u32[]{:S(2)}) %all-to-all-start.4) | async-done | bytes 1048608 | tf_op jit(solution)/shard_map/all_to_all | solution.py:36
  163.5 4.9 %all-to-all-start.5 = ((bf16[4,136,256]{2,1,0:T(8,128)(2,1)}), bf16[4,136,256]{2,1,0:T(8,128)(2,1)S(1)}, u32[]{:S(2)}, u32[]{:S(2)}) async-start(bf16[4,136,256]{2,1,0:T(8,128)(2,1)} %broadcast_in_dim.173), calls=%async_computation.5 | async-start | bytes 557056 | tf_op jit(solution)/shard_map/all_to_all | solution.py:36
  168.7 5.1 %all-to-all-done.5 = bf16[4,136,256]{2,1,0:T(8,128)(2,1)S(1)} async-done(((bf16[4,136,256]{2,1,0:T(8,128)(2,1)}), bf16[4,136,256]{2,1,0:T(8,128)(2,1)S(1)}, u32[]{:S(2)}, u32[]{:S(2)}) %all-to-all-start.5) | async-done | bytes 278560 | tf_op jit(solution)/shard_map/all_to_all | solution.py:36
  174.8 3.5 %all-to-all-start.6 = ((bf16[8,136,256]{2,1,0:T(8,128)(2,1)}), bf16[8,136,256]{2,1,0:T(8,128)(2,1)S(1)}, u32[]{:S(2)}, u32[]{:S(2)}) async-start(bf16[8,136,256]{2,1,0:T(8,128)(2,1)} %broadcast_in_dim.175), calls=%async_computation.6 | async-start | bytes 1114112 | tf_op jit(solution)/shard_map/all_to_all | solution.py:36
  178.4 5.0 %fusion.5 = f32[2,64,128]{2,1,0:T(8,128)S(1)} fusion(f32[2,64,128,64]{2,3,1,0:T(8,128)} %get-tuple-element.289, f32[2,64,128]{2,1,0:T(8,128)S(1)} %copy-done.20, f32[2,64,64]{2,1,0:T(8,128)S(1)} %copy.105), kind=kLoop, calls=%fused_computation.13 | loop fusion | flops 3129344 | bytes 4358144 | tf_op jit(solution)/shard_map/vmap(nts,nsd,ntsd->ntd)/dot_general | solution.py:96
  183.6 1.4 convolution_convert_fusion
  185.0 2.0 multiply_reduce_fusion
  187.0 6.0 %all-to-all-done.6 = bf16[8,136,256]{2,1,0:T(8,128)(2,1)S(1)} async-done(((bf16[8,136,256]{2,1,0:T(8,128)(2,1)}), bf16[8,136,256]{2,1,0:T(8,128)(2,1)S(1)}, u32[]{:S(2)}, u32[]{:S(2)}) %all-to-all-start.6) | async-done | bytes 557088 | tf_op jit(solution)/shard_map/all_to_all | solution.py:36
  193.0 5.0 %all-to-all-start.3 = ((bf16[32,64,256]{2,1,0:T(8,128)(2,1)}), bf16[32,64,256]{2,1,0:T(8,128)(2,1)S(1)}, u32[]{:S(2)}, u32[]{:S(2)}) async-start(bf16[32,64,256]{2,1,0:T(8,128)(2,1)} %bitcast.30), calls=%async_computation.3 | async-start | bytes 2097152 | tf_op jit(solution)/shard_map/all_to_all | solution.py:259
  201.6 20.1 %all-to-all-done.3 = bf16[32,64,256]{2,1,0:T(8,128)(2,1)S(1)} async-done(((bf16[32,64,256]{2,1,0:T(8,128)(2,1)}), bf16[32,64,256]{2,1,0:T(8,128)(2,1)S(1)}, u32[]{:S(2)}, u32[]{:S(2)}) %all-to-all-start.3) | async-done | bytes 1048608 | tf_op jit(solution)/shard_map/all_to_all | solution.py:259
  (189 shorter events, 28.2 us)
Async XLA Ops:
  0.6 182.9 %copy-start = (bf16[128,256]{1,0:T(8,128)(2,1)S(1)}, bf16[128,256]{1,0:T(8,128)(2,1)}, u32[]{:S(2)}) copy-start(bf16[128,256]{1,0:T(8,128)(2,1)} %param.28) | copy-start | bytes 196612
  0.6 5.5 %copy-start.2 = (bf16[128,2048]{1,0:T(8,128)(2,1)S(1)}, bf16[128,2048]{1,0:T(8,128)(2,1)}, u32[]{:S(2)}) copy-start(bf16[128,2048]{1,0:T(8,128)(2,1)} %param.19) | copy-start | bytes 1572868
  0.7 5.5 %copy-start.6 = (bf16[128,2048]{1,0:T(8,128)(2,1)S(1)}, bf16[128,2048]{1,0:T(8,128)(2,1)}, u32[]{:S(2)}) copy-start(bf16[128,2048]{1,0:T(8,128)(2,1)} %param.21) | copy-start | bytes 1572868
  9.0 13.6 %copy-start.31 = (f32[128,128]{1,0:T(8,128)S(1)}, f32[128,128]{1,0:T(8,128)}, u32[]{:S(2)}) copy-start(f32[128,128]{1,0:T(8,128)} %param.32) | copy-start | bytes 196612
  9.0 15.6 %copy-start.13 = (bf16[128,256]{1,0:T(8,128)(2,1)S(1)}, bf16[128,256]{1,0:T(8,128)(2,1)}, u32[]{:S(2)}) copy-start(bf16[128,256]{1,0:T(8,128)(2,1)} %param.31) | copy-start | bytes 196612
  9.0 15.6 %copy-start.18 = (bf16[128,128]{1,0:T(8,128)(2,1)S(1)}, bf16[128,128]{1,0:T(8,128)(2,1)}, u32[]{:S(2)}) copy-start(bf16[128,128]{1,0:T(8,128)(2,1)} %param.30) | copy-start | bytes 98308
  9.0 54.0 %copy-start.3 = (bf16[1,2048,128]{2,1,0:T(8,128)(2,1)S(1)}, bf16[1,2048,128]{2,1,0:T(8,128)(2,1)}, u32[]{:S(2)}) copy-start(bf16[1,2048,128]{2,1,0:T(8,128)(2,1)} %param.25) | copy-start | bytes 1572868
  9.0 52.0 %all-to-all-start = ((bf16[32,24,1024]{2,1,0:T(8,128)(2,1)}), bf16[32,24,1024]{2,1,0:T(8,128)(2,1)S(1)}, u32[]{:S(2)}, u32[]{:S(2)}) async-start(bf16[32,24,1024]{2,1,0:T(8,128)(2,1)} %bitcast.398), calls=%async_computation | async-start | bytes 3145728 | tf_op jit(solution)/shard_map/all_to_all | solution.py:170
  22.6 43.2 %copy-start.28 = (bf16[128,128]{1,0:T(8,128)(2,1)S(1)}, bf16[128,128]{1,0:T(8,128)(2,1)}, u32[]{:S(2)}) copy-start(bf16[128,128]{1,0:T(8,128)(2,1)} %param.29) | copy-start | bytes 98308
  61.0 5.7 %collective-permute-start = (bf16[768,1024]{1,0:T(8,128)(2,1)S(1)}, bf16[768,1024]{1,0:T(8,128)(2,1)}, u32[]{:S(2)}, u32[]{:S(2)}) collective-permute-start(bf16[768,1024]{1,0:T(8,128)(2,1)S(1)} %bitcast.381), channel_id=1, source_target_pairs={{0,1},{1,0},{2,3},{3,2},{4,5},{5,4},{6,7},{7,6},{8,9},{9,8},{10,11... | collective-permute-start | bytes 4718600 | tf_op jit(solution)/shard_map/ppermute | solution.py:171
  65.9 21.9 %copy-start.11 = (f32[128,128]{1,0:T(8,128)}, f32[128,128]{1,0:T(8,128)S(1)}, u32[]{:S(2)}) copy-start(f32[128,128]{1,0:T(8,128)S(1)} %convert_multiply_fusion.17) | copy-start | bytes 196612
  73.5 4.5 %collective-permute-start.1 = (bf16[384,1024]{1,0:T(8,128)(2,1)}, bf16[384,1024]{1,0:T(8,128)(2,1)}, u32[]{:S(2)}, u32[]{:S(2)}) collective-permute-start(bf16[384,1024]{1,0:T(8,128)(2,1)} %convolution_convert_fusion.2), channel_id=1, source_target_pairs={{0,1},{1,0},{2,3},{3,2},{4,5},{5,4},{6,7},{7,6},{8,9},{9,8},{10,11... | collective-permute-start | bytes 2359304 | tf_op jit(solution)/shard_map/ppermute | solution.py:209
  79.6 8.2 %copy-start.21 = (f32[2,128,64]{1,2,0:T(8,128)S(1)}, f32[2,128,64]{1,2,0:T(8,128)}, u32[]{:S(2)}) copy-start(f32[2,128,64]{1,2,0:T(8,128)} %get-tuple-element.296) | copy-start | bytes 196612
  80.7 30.8 %all-to-all-start.1 = ((bf16[8,384,128]{2,1,0:T(8,128)(2,1)}), bf16[8,384,128]{2,1,0:T(8,128)(2,1)S(1)}, u32[]{:S(2)}, u32[]{:S(2)}) async-start(bf16[8,384,128]{2,1,0:T(8,128)(2,1)} %bitcast.389), calls=%async_computation.1 | async-start | bytes 1572864 | tf_op jit(solution)/shard_map/all_to_all | solution.py:212
  97.1 30.7 %copy-start.32 = (bf16[64,256]{1,0:T(8,128)(2,1)S(1)}, bf16[64,256]{1,0:T(8,128)(2,1)}, u32[]{:S(2)}) copy-start(bf16[64,256]{1,0:T(8,128)(2,1)} %param.27) | copy-start | bytes 98308
  112.3 15.5 %all-to-all-start.2 = ((bf16[32,12,128]{2,1,0:T(8,128)(2,1)}), bf16[32,12,128]{2,1,0:T(8,128)(2,1)S(1)}, u32[]{:S(2)}, u32[]{:S(2)}) async-start(bf16[32,12,128]{2,1,0:T(8,128)(2,1)} %reshape.965), calls=%async_computation.2 | async-start | bytes 262144 | tf_op jit(solution)/shard_map/all_to_all | solution.py:233
  120.7 13.9 %copy-start.10 = (bf16[1024,128]{1,0:T(8,128)(2,1)S(1)}, bf16[1024,128]{1,0:T(8,128)(2,1)}, u32[]{:S(2)}) copy-start(bf16[1024,128]{1,0:T(8,128)(2,1)} %get-tuple-element.275) | copy-start | bytes 786436
  129.0 6.5 %copy-start.17 = (bf16[256,1024]{1,0:T(8,128)(2,1)S(1)}, bf16[256,1024]{1,0:T(8,128)(2,1)}, u32[]{:S(2)}) copy-start(bf16[256,1024]{1,0:T(8,128)(2,1)} %convolution_convert_fusion.3) | copy-start | bytes 1572868
  129.0 32.6 %all-to-all-start.4 = ((bf16[32,64,256]{2,1,0:T(8,128)(2,1)}), bf16[32,64,256]{2,1,0:T(8,128)(2,1)S(1)}, u32[]{:S(2)}, u32[]{:S(2)}) async-start(bf16[32,64,256]{2,1,0:T(8,128)(2,1)} %broadcast_in_dim.169), calls=%async_computation.4 | async-start | bytes 2097152 | tf_op jit(solution)/shard_map/all_to_all | solution.py:36
  135.5 17.3 %copy-start.30 = (f32[2048]{0:T(1024)S(1)}, f32[2048]{0:T(1024)}, u32[]{:S(2)}) copy-start(f32[2048]{0:T(1024)} %param.20) | copy-start | bytes 24580
  135.5 17.3 %copy-start.34 = (f32[128]{0:T(128)S(1)}, f32[128]{0:T(128)}, u32[]{:S(2)}) copy-start(f32[128]{0:T(128)} %copy-done.33) | copy-start | bytes 1540
  135.5 17.6 %copy-start.7 = (bf16[128,2048]{1,0:T(8,128)(2,1)S(1)}, bf16[128,2048]{1,0:T(8,128)(2,1)}, u32[]{:S(2)}) copy-start(bf16[128,2048]{1,0:T(8,128)(2,1)} %param.21) | copy-start | bytes 1572868
  153.1 8.8 %copy-start.12 = (f32[128,128]{1,0:T(8,128)S(1)}, f32[128,128]{1,0:T(8,128)}, u32[]{:S(2)}) copy-start(f32[128,128]{1,0:T(8,128)} %copy-done.11) | copy-start | bytes 196612
  153.5 8.7 %copy-start.37 = (f32[2,1,128]{2,1,0:T(1,128)S(1)}, f32[2,1,128]{2,1,0:T(1,128)}, u32[]{:S(2)}) copy-start(f32[2,1,128]{2,1,0:T(1,128)} %get-tuple-element.408) | copy-start | bytes 3076
  162.2 6.3 %copy-start.14 = (bf16[128,256]{1,0:T(8,128)(2,1)S(1)}, bf16[128,256]{1,0:T(8,128)(2,1)}, u32[]{:S(2)}) copy-start(bf16[128,256]{1,0:T(8,128)(2,1)} %param.31) | copy-start | bytes 196612
  163.5 14.8 %copy-start.20 = (f32[2,64,128]{2,1,0:T(8,128)S(1)}, f32[2,64,128]{2,1,0:T(8,128)}, u32[]{:S(2)}) copy-start(f32[2,64,128]{2,1,0:T(8,128)} %get-tuple-element.297) | copy-start | bytes 196612
  163.5 10.2 %all-to-all-start.5 = ((bf16[4,136,256]{2,1,0:T(8,128)(2,1)}), bf16[4,136,256]{2,1,0:T(8,128)(2,1)S(1)}, u32[]{:S(2)}, u32[]{:S(2)}) async-start(bf16[4,136,256]{2,1,0:T(8,128)(2,1)} %broadcast_in_dim.173), calls=%async_computation.5 | async-start | bytes 557056 | tf_op jit(solution)/shard_map/all_to_all | solution.py:36
  174.8 18.2 %all-to-all-start.6 = ((bf16[8,136,256]{2,1,0:T(8,128)(2,1)}), bf16[8,136,256]{2,1,0:T(8,128)(2,1)S(1)}, u32[]{:S(2)}, u32[]{:S(2)}) async-start(bf16[8,136,256]{2,1,0:T(8,128)(2,1)} %broadcast_in_dim.175), calls=%async_computation.6 | async-start | bytes 1114112 | tf_op jit(solution)/shard_map/all_to_all | solution.py:36
  178.4 5.0 %copy-start.15 = (bf16[2,1,128,256]{3,2,1,0:T(8,128)(2,1)S(1)}, bf16[2,1,128,256]{3,2,1,0:T(8,128)(2,1)}, u32[]{:S(2)}) copy-start(bf16[2,1,128,256]{3,2,1,0:T(8,128)(2,1)} %get-tuple-element.142) | copy-start | bytes 393220
  187.0 11.4 %copy-start.19 = (bf16[128,128]{1,0:T(8,128)(2,1)S(1)}, bf16[128,128]{1,0:T(8,128)(2,1)}, u32[]{:S(2)}) copy-start(bf16[128,128]{1,0:T(8,128)(2,1)} %param.30) | copy-start | bytes 98308
  187.0 11.4 %copy-start.29 = (bf16[128,128]{1,0:T(8,128)(2,1)S(1)}, bf16[128,128]{1,0:T(8,128)(2,1)}, u32[]{:S(2)}) copy-start(bf16[128,128]{1,0:T(8,128)(2,1)} %param.29) | copy-start | bytes 98308
  193.0 28.6 %all-to-all-start.3 = ((bf16[32,64,256]{2,1,0:T(8,128)(2,1)}), bf16[32,64,256]{2,1,0:T(8,128)(2,1)S(1)}, u32[]{:S(2)}, u32[]{:S(2)}) async-start(bf16[32,64,256]{2,1,0:T(8,128)(2,1)} %bitcast.30), calls=%async_computation.3 | async-start | bytes 2097152 | tf_op jit(solution)/shard_map/all_to_all | solution.py:259
  (18 other events, 53.3 us)
